TPU v7x, 32 devices: a whole 2x2x4 slice. The times are simulated.
32 devices in a mesh: ep: 4 (over z), tp: 8 (over y, x, core).
Axes of the slice: x: 2, y: 2, z: 4, core: 2. Of those that a mesh axis runs over, the one named last changes fastest.
Arguments:
- tokens: bfloat16 [512, 2048], P('ep', 'tp'), may hold values from -6 to 6
- out_grad: bfloat16 [512, 2048], P('ep', 'tp'), may hold values from -6 to 6
- routes: int32 [512, 2], P('ep'), may hold values from 0 to 3, all different within a row; in each aligned block of 128 rows (0 to 127, 128 to 255, ...) at most 96 rows name the same one
- gates: float32 [512, 2], P('ep'), may hold values from 0.1 to 0.9
- gate_weight: bfloat16 [4, 2048, 5632], P('ep', None, 'tp'), may hold values from -0.125 to 0.125
- up_weight: bfloat16 [4, 2048, 5632], P('ep', None, 'tp'), may hold values from -0.125 to 0.125
- down_weight: bfloat16 [4, 5632, 2048], P('ep', 'tp'), may hold values from -0.078125 to 0.078125
Outputs:
- tokens_grad: bfloat16 [512, 2048], P('ep', 'tp')
- gates_grad: float32 [512, 2], P(('ep', 'tp'))
- gate_weight_grad: bfloat16 [4, 2048, 5632], P('ep', None, 'tp')
- up_weight_grad: bfloat16 [4, 2048, 5632], P('ep', None, 'tp')
- down_weight_grad: bfloat16 [4, 5632, 2048], P('ep', 'tp')
Inputs may be any that keep to these rules, and one draw needn't show every extreme that they name: `routes`: the 2 experts of a token differ. In each aligned block of 128 rows (the tokens of one index of ep) no expert is named by more than 96 rows, a bound that some block reaches.
All inputs are finite; a program needn't handle non-finite values.
Results may differ from a plain program's by a relative error of at most 0.029.
Values may be sent and summed in bfloat16 or wider, within the bound.
A program may use at most 64 MiB of HBM per device.

v0:
```python
import functools

import jax
import jax.numpy as jnp
from jax import lax
from jax.experimental import pallas as pl
from jax.experimental.pallas import tpu as pltpu
from jax.sharding import PartitionSpec as P

MESH = pl.DeviceIdType.MESH
BF16 = jnp.bfloat16
F32 = jnp.float32
VMEM_BYTES = 60 * 1024 * 1024


def dot_nn(a, b):
    return lax.dot_general(a, b, (((1,), (0,)), ((), ())), preferred_element_type=F32)


def dot_nt(a, b):
    return lax.dot_general(a, b, (((1,), (1,)), ((), ())), preferred_element_type=F32)


def dot_tn(a, b):
    return lax.dot_general(a, b, (((0,), (0,)), ((), ())), preferred_element_type=F32)


def flip(t, bit):
    return t + bit - 2 * bit * lax.rem(lax.div(t, bit), 2)


def exchange_kernel(
    ep, tp, cap,
    tok_ref, og_ref, routes_ref, gates_ref, wg_hbm, wu_hbm, wd_hbm,
    tg_ref, gg_ref, xo_hbm, co_hbm, ho_hbm, gpo_hbm, upo_hbm,
    wg, wu, wd, sx, sc, xs, cs, comb_ref, pick_ref,
    pg, pu, hg, hid, gp, up, hid_t, gp_t, up_t,
    psib, rsib, pown, rown, mine, tsum, back, dsend, drecv, dsum, dback,
    wsem, osem,
    zs, zr, ns, nr, ds_, dr, ss, sr,
    bss, bsr, rs, rr, zbs, zbr, dts, dtr, dzs, dzr,
):
    me_e = lax.axis_index("ep")
    me_t = lax.axis_index("tp")
    sib = flip(me_t, 1)
    nbr = (flip(me_t, 2), flip(me_t, 4))
    diag = flip(nbr[0], 4)
    slots = ep * cap
    tok_dev, dw = tok_ref.shape
    fw = wg.shape[0]

    def rdma(src, dst, s_sem, r_sem, e, t):
        return pltpu.make_async_remote_copy(
            src_ref=src, dst_ref=dst, send_sem=s_sem, recv_sem=r_sem,
            device_id={"ep": e, "tp": t}, device_id_type=MESH,
        )

    loads = [
        pltpu.make_async_copy(src.at[0], dst, wsem.at[i])
        for i, (src, dst) in enumerate(((wg_hbm, wg), (wu_hbm, wu), (wd_hbm, wd)))
    ]
    for load in loads:
        load.start()

    barrier = pltpu.get_barrier_semaphore()
    for r in range(1, ep):
        pl.semaphore_signal(
            barrier, inc=1, device_id={"ep": lax.rem(me_e + r, ep), "tp": me_t}, device_id_type=MESH)
    for r in range(1, tp):
        pl.semaphore_signal(
            barrier, inc=1, device_id={"ep": me_e, "tp": lax.rem(me_t + r, tp)}, device_id_type=MESH)

    expert = [routes_ref[k : k + 1, :].astype(F32) for k in range(2)]
    group = lax.broadcasted_iota(jnp.int32, (16, tok_dev), 0).astype(F32)
    oh = [jnp.where(expert[k] == group, 1.0, 0.0) for k in range(2)]
    row_id = lax.broadcasted_iota(jnp.int32, (tok_dev, tok_dev), 0)
    col_id = lax.broadcasted_iota(jnp.int32, (tok_dev, tok_dev), 1)
    above = jnp.where(row_id < col_id, 1.0, 0.0).astype(BF16)
    before = dot_nn((oh[0] + oh[1]).astype(BF16), above)
    rank = [
        jnp.sum(before * oh[0], axis=0, keepdims=True),
        jnp.sum((before + oh[0]) * oh[1], axis=0, keepdims=True),
    ]
    slot_id = lax.broadcasted_iota(jnp.int32, (slots, tok_dev), 0).astype(F32)
    slot_gate = jnp.zeros((slots, 1), F32)
    both = jnp.zeros((slots, tok_dev), F32)
    for k in range(2):
        pick = jnp.where(expert[k] * float(cap) + rank[k] == slot_id, 1.0, 0.0)
        pick_ref[k] = pick
        both = both + pick
        slot_gate = slot_gate + jnp.sum(pick * gates_ref[k : k + 1, :], axis=1, keepdims=True)
    select = both.astype(BF16)
    comb_ref[...] = select
    sx[...] = dot_nn(select, tok_ref[...]).astype(BF16)
    sc[...] = (slot_gate * dot_nn(select, og_ref[...])).astype(BF16)

    pl.semaphore_wait(barrier, ep - 1 + tp - 1)

    def rows_of(s):
        return pl.ds(pl.multiple_of(s * cap, cap), cap)

    sent, big = (sx, sc), (xs, cs)
    src_of = [lax.rem(me_e + ep - r, ep) for r in range(ep)]
    n_chunk = 2 * ep
    sends = []

    def start(copy):
        copy.start()
        sends.append(copy)
        return copy

    z_copy = {}
    for a in range(2):
        for r in range(1, ep):
            to = lax.rem(me_e + r, ep)
            z_copy[a * ep + r] = start(rdma(
                sent[a].at[rows_of(to)], big[a].at[me_t, rows_of(me_e)],
                zs.at[a * ep + r], zr.at[a * ep + r], to, me_t))
    for a in range(2):
        big[a][me_t, rows_of(me_e), :] = sent[a][rows_of(me_e), :]

    n_copy, d_copy, s_copy = {}, {}, {}

    def chunk(i, t):
        return big[i // ep].at[t, rows_of(src_of[i % ep])]

    def to_sibling(i, kind, t):
        s_copy[i, kind] = start(rdma(
            chunk(i, t), chunk(i, t), ss.at[i * 4 + kind], sr.at[i * 4 + kind], me_e, sib))

    def stage_a(i):
        if i in z_copy:
            z_copy[i].wait_recv()
        for d in range(2):
            n_copy[i, d] = start(rdma(
                chunk(i, me_t), chunk(i, me_t), ns.at[i * 2 + d], nr.at[i * 2 + d], me_e, nbr[d]))
        to_sibling(i, 0, me_t)

    def stage_b(i):
        for d in range(2):
            n_copy[i, d].wait_recv()
            if i % 2 == d:
                d_copy[i] = start(rdma(
                    chunk(i, nbr[d]), chunk(i, nbr[d]), ds_.at[i], dr.at[i], me_e, nbr[1 - d]))
            to_sibling(i, 1 + d, nbr[d])

    def stage_c(i):
        d_copy[i].wait_recv()
        to_sibling(i, 3, diag)

    def settle(a):
        for i in range(a * ep, (a + 1) * ep):
            for kind in range(4):
                s_copy[i, kind].wait_recv()

    def first_half(lo, hi):
        @pl.loop(lo, hi)
        def _(j):
            part = pl.ds(pl.multiple_of(j * dw, dw), dw)
            x = xs[j]
            pg[...] += dot_nt(x, wg[:, part])
            pu[...] += dot_nt(x, wu[:, part])

    outs = []

    def put(src, dst, k):
        copy = pltpu.make_async_copy(src, dst, osem.at[k])
        copy.start()
        outs.append(copy)

    pg[...] = jnp.zeros_like(pg)
    pu[...] = jnp.zeros_like(pu)
    hg[...] = jnp.zeros_like(hg)
    for i in range(n_chunk + 2):
        if i < n_chunk:
            stage_a(i)
        if 1 <= i <= n_chunk:
            stage_b(i - 1)
        if i >= 2:
            stage_c(i - 2)
        late = i - (ep + 2)
        if late == 0:
            settle(0)
            put(xs, xo_hbm, 0)
            loads[0].wait()
            loads[1].wait()
        if late >= 0:
            first_half(late * tp // ep, (late + 1) * tp // ep)
    settle(1)
    put(cs, co_hbm, 1)
    loads[2].wait()

    @pl.loop(0, tp)
    def _(j):
        part = pl.ds(pl.multiple_of(j * dw, dw), dw)
        hg[...] += dot_nt(cs[j], wd[:, part])

    block = 16

    @pl.loop(0, slots // block)
    def _(b):
        at = pl.ds(pl.multiple_of(b * block, block), block)
        g, u, h = pg[at, :], pu[at, :], hg[at, :]
        sig = jax.nn.sigmoid(g)
        act = g * sig
        hidden = (act * u).astype(BF16)
        hid[at, :] = hidden
        gp[at, :] = (h * u * sig * (1.0 + g * (1.0 - sig))).astype(BF16)
        up[at, :] = (h * act).astype(BF16)
        pg[at, :] = hidden.astype(F32) * h

    def piece(t):
        part = pl.ds(pl.multiple_of(t * dw, dw), dw)
        return dot_nn(gp[...], wg[:, part]) + dot_nn(up[...], wu[:, part])

    ones = jnp.ones((8, fw), F32)
    tile_row = lax.broadcasted_iota(jnp.int32, (8, 128), 0)
    tile = jnp.zeros((8, 128), F32)
    for s in range(ep):
        sums = lax.dot_general(
            ones, pg[s * cap : (s + 1) * cap, :], (((1,), (1,)), ((), ())),
            precision=lax.Precision.HIGHEST, preferred_element_type=F32)
        if cap < 128:
            sums = jnp.concatenate([sums, jnp.zeros((8, 128 - cap), F32)], axis=1)
        tile = jnp.where(tile_row == s, sums, tile)
    dsend[...] = tile
    t_copy = []
    for r in range(1, tp):
        t_copy.append(start(rdma(
            dsend, drecv.at[r - 1], dts.at[r - 1], dtr.at[r - 1], me_e, lax.rem(me_t + r, tp))))

    chips = (diag, nbr[0], nbr[1], me_t)
    b_copy = []
    for q in range(4):
        psib[q] = piece(flip(chips[q], 1)).astype(BF16)
        b_copy.append(start(rdma(psib.at[q], rsib.at[q], bss.at[q], bsr.at[q], me_e, sib)))
    for q in range(3):
        own = piece(chips[q])
        b_copy[q].wait_recv()
        pown[q] = (own + rsib[q].astype(F32)).astype(BF16)
    order = list(range(1, ep)) + [0]
    r_copy = {}
    for r in order:
        for q in range(3):
            at = rows_of(lax.rem(me_e + r, ep))
            r_copy[r, q] = start(rdma(
                pown.at[q, at], rown.at[q, at], rs.at[r * 3 + q], rr.at[r * 3 + q], me_e, chips[q]))

    dots = dsend[...]
    for copy_index, copy in enumerate(t_copy):
        copy.wait_recv()
        dots = dots + drecv[copy_index]
    dsum[...] = dots
    dz_copy = []
    for r in range(1, ep):
        to = lax.rem(me_e + r, ep)
        dz_copy.append(start(rdma(dsum, dback.at[me_e], dzs.at[r - 1], dzr.at[r - 1], to, me_t)))
    dback[me_e] = dots

    for k, (rows, flat, out) in enumerate(((hid, hid_t, ho_hbm), (gp, gp_t, gpo_hbm), (up, up_t, upo_hbm))):
        flat[...] = rows[...].T
        put(flat, out, 2 + k)

    own = piece(me_t)
    b_copy[3].wait_recv()
    mine[...] = own + rsib[3].astype(F32)
    zb_copy = []
    for r in order:
        to = lax.rem(me_e + r, ep)
        at = rows_of(to)
        total = mine[at, :]
        for q in range(3):
            r_copy[r, q].wait_recv()
            total = total + rown[q, at, :].astype(F32)
        tsum[at, :] = total.astype(BF16)
        if r:
            zb_copy.append(start(rdma(
                tsum.at[at], back.at[rows_of(me_e)], zbs.at[r - 1], zbr.at[r - 1], to, me_t)))
        else:
            back[at, :] = tsum[at, :]

    for copy in dz_copy:
        copy.wait_recv()
    share = tok_dev // tp
    own_row = lax.broadcasted_iota(jnp.int32, (tok_dev, share), 0)
    own_col = lax.broadcasted_iota(jnp.int32, (tok_dev, share), 1) + me_t * share
    own_pick = jnp.where(own_row == own_col, 1.0, 0.0)
    exact = dict(precision=lax.Precision.HIGHEST, preferred_element_type=F32)
    mine_row = lax.broadcasted_iota(jnp.int32, (8, 128), 0) == me_e
    grads = []
    for k in range(2):
        total = jnp.zeros((8, tok_dev), F32)
        for s in range(ep):
            held = jnp.where(mine_row, dback[s], 0.0)[:, 0:cap]
            total = total + jnp.dot(held, pick_ref[k, s * cap : (s + 1) * cap, :], **exact)
        grads.append(jnp.sum(total, axis=0, keepdims=True) / gates_ref[k : k + 1, :])
    shares = jnp.concatenate([*grads, jnp.zeros((6, tok_dev), F32)], axis=0)
    gg_ref[...] = jnp.dot(shares, own_pick, **exact)[0:2, :]

    for copy in zb_copy:
        copy.wait_recv()
    tg_ref[...] = dot_tn(comb_ref[...], back[...]).astype(BF16)
    for copy in sends:
        copy.wait_send()
    for copy in outs:
        copy.wait()


def weight_kernel(x_ref, c_ref, hid_ref, gp_ref, up_ref, gg_ref, ug_ref, dg_ref):
    x = x_ref[...]
    gg_ref[...] = dot_nn(gp_ref[...], x).astype(BF16)
    ug_ref[...] = dot_nn(up_ref[...], x).astype(BF16)
    dg_ref[...] = dot_nn(hid_ref[...], c_ref[...]).astype(BF16)


def fused(tokens, out_grad, routes, gates, gate_weight, up_weight, down_weight):
    tok_dev, top_k = routes.shape
    ep = lax.axis_size("ep")
    tp = lax.axis_size("tp")
    cap = (3 * tok_dev + ep - 1) // ep
    slots = ep * cap
    dw = tokens.shape[1]
    model = gate_weight.shape[1]
    fw = gate_weight.shape[2]
    share = tok_dev // tp
    vmem = pl.BlockSpec(memory_space=pltpu.VMEM)
    any_ = pl.BlockSpec(memory_space=pl.ANY)
    dma = lambda n: pltpu.SemaphoreType.DMA((n,))
    wide = jax.ShapeDtypeStruct((tp, slots, dw), BF16)
    part = jax.ShapeDtypeStruct((fw, slots), BF16)
    flops = 10 * slots * model * fw
    tokens_grad, gates_grad, xs, cs, hid, gp, up = pl.pallas_call(
        functools.partial(exchange_kernel, ep, tp, cap),
        out_shape=(
            jax.ShapeDtypeStruct((tok_dev, dw), BF16),
            jax.ShapeDtypeStruct((top_k, share), F32),
            wide, wide, part, part, part,
        ),
        in_specs=[vmem] * 4 + [any_] * 3,
        out_specs=[vmem, vmem] + [any_] * 5,
        scratch_shapes=[
            pltpu.VMEM((fw, model), BF16),
            pltpu.VMEM((fw, model), BF16),
            pltpu.VMEM((fw, model), BF16),
            pltpu.VMEM((slots, dw), BF16),
            pltpu.VMEM((slots, dw), BF16),
            pltpu.VMEM((tp, slots, dw), BF16),
            pltpu.VMEM((tp, slots, dw), BF16),
            pltpu.VMEM((slots, tok_dev), BF16),
            pltpu.VMEM((2, slots, tok_dev), F32),
            pltpu.VMEM((slots, fw), F32),
            pltpu.VMEM((slots, fw), F32),
            pltpu.VMEM((slots, fw), F32),
            pltpu.VMEM((slots, fw), BF16),
            pltpu.VMEM((slots, fw), BF16),
            pltpu.VMEM((slots, fw), BF16),
            pltpu.VMEM((fw, slots), BF16),
            pltpu.VMEM((fw, slots), BF16),
            pltpu.VMEM((fw, slots), BF16),
            pltpu.VMEM((4, slots, dw), BF16),
            pltpu.VMEM((4, slots, dw), BF16),
            pltpu.VMEM((3, slots, dw), BF16),
            pltpu.VMEM((3, slots, dw), BF16),
            pltpu.VMEM((slots, dw), F32),
            pltpu.VMEM((slots, dw), BF16),
            pltpu.VMEM((slots, dw), BF16),
            pltpu.VMEM((8, 128), F32),
            pltpu.VMEM((tp - 1, 8, 128), F32),
            pltpu.VMEM((8, 128), F32),
            pltpu.VMEM((ep, 8, 128), F32),
            dma(3), dma(5),
            dma(2 * ep), dma(2 * ep), dma(4 * ep), dma(4 * ep), dma(2 * ep), dma(2 * ep),
            dma(8 * ep), dma(8 * ep),
            dma(4), dma(4), dma(3 * ep), dma(3 * ep), dma(ep), dma(ep),
            dma(tp), dma(tp), dma(ep), dma(ep),
        ],
        compiler_params=pltpu.CompilerParams(
            collective_id=0, has_side_effects=True, vmem_limit_bytes=VMEM_BYTES),
        cost_estimate=pl.CostEstimate(flops=flops, bytes_accessed=6 * model * fw, transcendentals=0),
    )(tokens, out_grad, routes.T, gates.T, jnp.swapaxes(gate_weight, 1, 2),
      jnp.swapaxes(up_weight, 1, 2), down_weight)
    whole = pl.BlockSpec((fw, slots), lambda j: (0, 0))
    slab = pl.BlockSpec((None, slots, dw), lambda j: (j, 0, 0))
    tall = pl.BlockSpec((None, fw, dw), lambda j: (0, 0, j))
    gate_grad, up_grad, down_grad = pl.pallas_call(
        weight_kernel,
        grid=(tp,),
        out_shape=(
            jax.ShapeDtypeStruct((1, fw, model), BF16),
            jax.ShapeDtypeStruct((1, fw, model), BF16),
            jax.ShapeDtypeStruct((1, fw, model), BF16),
        ),
        in_specs=[slab, slab, whole, whole, whole],
        out_specs=[tall, tall, tall],
        compiler_params=pltpu.CompilerParams(vmem_limit_bytes=VMEM_BYTES),
        cost_estimate=pl.CostEstimate(
            flops=6 * slots * model * fw, bytes_accessed=6 * model * fw, transcendentals=0),
    )(xs, cs, hid, gp, up)
    return (tokens_grad, gates_grad.T, jnp.swapaxes(gate_grad, 1, 2), jnp.swapaxes(up_grad, 1, 2), down_grad)


def fits_fused(ep, tp, tokens, routes, gate_weight):
    cap = (3 * routes.shape[0] + ep - 1) // ep
    return (
        tp == 8 and 2 <= ep <= 8 and tp % ep == 0 and cap % 16 == 0 and cap <= 128
        and tokens.shape[1] % 128 == 0 and routes.shape[1] == 2
        and routes.shape[0] % (8 * tp) == 0
        and gate_weight.shape[2] % 16 == 0
    )


def expert_grads(rows, cotan, w_gate, w_up, w_down):
    pre_gate = jnp.dot(rows, w_gate, preferred_element_type=jnp.float32)
    pre_up = jnp.dot(rows, w_up, preferred_element_type=jnp.float32)
    activated = jax.nn.silu(pre_gate)
    hidden = (activated * pre_up).astype(jnp.bfloat16)
    hid_grad = jnp.dot(cotan, w_down.T, preferred_element_type=jnp.float32)
    sigmoid_gate = jax.nn.sigmoid(pre_gate)
    gate_part = (hid_grad * pre_up * sigmoid_gate * (1.0 + pre_gate * (1.0 - sigmoid_gate))).astype(
        jnp.bfloat16
    )
    up_part = (hid_grad * activated).astype(jnp.bfloat16)
    slot_dots = jnp.sum(hidden.astype(jnp.float32) * hid_grad, axis=1)
    down_grad = jnp.dot(hidden.T, cotan, preferred_element_type=jnp.float32).astype(jnp.bfloat16)
    gate_grad = jnp.dot(rows.T, gate_part, preferred_element_type=jnp.float32).astype(jnp.bfloat16)
    up_grad = jnp.dot(rows.T, up_part, preferred_element_type=jnp.float32).astype(jnp.bfloat16)
    return (gate_part, up_part, slot_dots, gate_grad, up_grad, down_grad)


def on_device(tokens, out_grad, routes, gates, gate_weight, up_weight, down_weight):
    tok_dev, top_k = routes.shape
    ep_size = lax.axis_size("ep")
    tp_size = lax.axis_size("tp")
    if fits_fused(ep_size, tp_size, tokens, routes, gate_weight):
        return fused(tokens, out_grad, routes, gates, gate_weight, up_weight, down_weight)
    capacity = (3 * tok_dev + ep_size - 1) // ep_size
    buffer_rows = ep_size * capacity
    slice_width = tokens.shape[1]
    flat_expert = routes.reshape(-1)
    onehot = (flat_expert[:, None] == jnp.arange(ep_size, dtype=jnp.int32)[None, :]).astype(
        jnp.int32
    )
    slot_rank = jnp.sum((jnp.cumsum(onehot, axis=0) - onehot) * onehot, axis=1)
    slot_dest = flat_expert * capacity + slot_rank
    placed = jnp.arange(buffer_rows, dtype=jnp.int32)[:, None] == slot_dest[None, :]
    placed_float = placed.astype(jnp.float32)
    select = jnp.any(placed.reshape(buffer_rows, tok_dev, top_k), axis=2).astype(jnp.bfloat16)
    slot_gate = jnp.dot(placed_float, gates.reshape(-1), precision=lax.Precision.HIGHEST)
    sent_rows = jnp.dot(select, tokens, preferred_element_type=jnp.float32).astype(jnp.bfloat16)
    cotan_rows = jnp.dot(select, out_grad, preferred_element_type=jnp.float32)
    sent_cotan = (slot_gate[:, None] * cotan_rows).astype(jnp.bfloat16)
    recv_rows, recv_cotan = (
        lax.all_to_all(
            sent_rows.reshape(ep_size, capacity, slice_width),
            "ep",
            split_axis=0,
            concat_axis=0,
            tiled=True,
        ),
        lax.all_to_all(
            sent_cotan.reshape(ep_size, capacity, slice_width),
            "ep",
            split_axis=0,
            concat_axis=0,
            tiled=True,
        ),
    )
    whole_rows, whole_cotan = (
        lax.all_gather(recv_rows, "tp", axis=2, tiled=True),
        lax.all_gather(recv_cotan, "tp", axis=2, tiled=True),
    )
    model_width = whole_rows.shape[2]
    rows = whole_rows.reshape(buffer_rows, model_width)
    cotan = whole_cotan.reshape(buffer_rows, model_width)
    w_gate = gate_weight[0]
    w_up = up_weight[0]
    gate_part, up_part, slot_dots, gate_grad, up_grad, down_grad = expert_grads(
        rows, cotan, w_gate, w_up, down_weight[0]
    )
    partial_value = jnp.dot(gate_part, w_gate.T, preferred_element_type=jnp.float32)
    partial_value = (
        partial_value + jnp.dot(up_part, w_up.T, preferred_element_type=jnp.float32)
    ).astype(jnp.bfloat16)
    share = tok_dev // tp_size
    start = lax.axis_index("tp") * share
    summed = lax.psum(slot_dots, "tp")
    row_sums = lax.psum_scatter(
        partial_value.reshape(ep_size, capacity, model_width), "tp", scatter_dimension=2, tiled=True
    ).astype(jnp.float32)
    back_rows, back_dots = (
        lax.all_to_all(
            row_sums.astype(jnp.bfloat16), "ep", split_axis=0, concat_axis=0, tiled=True
        ).astype(row_sums.dtype),
        lax.all_to_all(
            summed.reshape(ep_size, capacity).astype(jnp.bfloat16),
            "ep",
            split_axis=0,
            concat_axis=0,
            tiled=True,
        ).astype(jnp.float32),
    )
    slot_rows = back_rows.reshape(buffer_rows, slice_width)[slot_dest]
    tokens_grad = jnp.sum(slot_rows.reshape(tok_dev, top_k, slice_width), axis=1).astype(
        jnp.bfloat16
    )
    token_dots = back_dots.reshape(buffer_rows)[slot_dest].reshape(tok_dev, top_k)
    own_dots = lax.dynamic_slice_in_dim(token_dots, start, share, 0)
    own_gates = lax.dynamic_slice_in_dim(gates, start, share, 0)
    gates_grad = own_dots / own_gates
    return (tokens_grad, gates_grad, gate_grad[None], up_grad[None], down_grad[None])


def solution(mesh):
    placed = (
        P("ep", "tp"),
        P("ep", "tp"),
        P("ep", None),
        P("ep", None),
        P("ep", None, "tp"),
        P("ep", None, "tp"),
        P("ep", "tp", None),
    )
    return jax.shard_map(
        on_device,
        mesh=mesh,
        in_specs=placed,
        out_specs=(
            P("ep", "tp"),
            P(("ep", "tp"), None),
            P("ep", None, "tp"),
            P("ep", None, "tp"),
            P("ep", "tp", None),
        ),
        check_vma=False,
    )
```

profile of v0, /device:TPU:0, one launch (start us, length us, event | category | flops | bytes accessed | tf_op | source)
XLA Modules:
  0.0 70.2 jit_solution(14166418024181531467)
XLA Ops:
  0.6 57.9 %shard_map.110 = (bf16[128,256]{1,0:T(8,128)(2,1)}, f32[2,16]{1,0:T(2,128)}, bf16[8,384,256]{2,1,0:T(8,128)(2,1)}, bf16[8,384,256]{2,1,0:T(8,128)(2,1)}, bf16[70...) custom-call(bf16[128,256]{1,0:T(8,128)(2,1)} %tok_ref.1, bf16[128,256]{1,0:T(8,128)(2,1)} %og_ref.1, ...), custom_call_target="tpu_custom_call" | custom-call | flops 5536481280 | bytes 8650752 | tf_op jit(solution)/shard_map/pallas_call | solution.py:332
  58.6 0.0 copy-start
  58.6 0.0 copy-start.1
  58.6 10.4 %shard_map.111 = (bf16[1,704,2048]{2,1,0:T(8,128)(2,1)}, bf16[1,704,2048]{2,1,0:T(8,128)(2,1)}, bf16[1,704,2048]{2,1,0:T(8,128)(2,1)}) custom-call(bf16[8,384,256]{2,1,0:T(8,128)(2,1)} %get-tuple-element.17.x_ref, bf16[8,384,256]{2,1,0:T(8,128)(2,1)} %get-tuple-element.18.c_ref, bf16[704,384]{1,0:T(8,128)(2,1)} %get-tuple-element.19.hid_ref, ...), custom_call_target="tpu_custom_call" | custom-call | flops 3321888768 | bytes 8650752 | tf_op jit(solution)/shard_map/pallas_call | solution.py:385
  69.0 0.0 copy-done
  69.0 0.6 copy.14
  69.6 0.0 copy-done.1
  69.6 0.6 copy.15
Async XLA Ops:
  58.6 10.4 %copy-start = (bf16[128,256]{1,0:T(8,128)(2,1)S(1)}, bf16[128,256]{1,0:T(8,128)(2,1)}, u32[]{:S(2)}) copy-start(bf16[128,256]{1,0:T(8,128)(2,1)} %get-tuple-element.30) | copy-start | bytes 196612
  58.6 11.0 %copy-start.1 = (f32[2,16]{1,0:T(2,128)S(1)}, f32[2,16]{1,0:T(2,128)}, u32[]{:S(2)}) copy-start(f32[2,16]{1,0:T(2,128)} %get-tuple-element.16) | copy-start | bytes 388
where the time goes:
time: 70.5 us; the launch traced here: 70.2 us
  Pallas kernels  68.3 us (97%)
  local copies, waits for them, and re-layouts  1.2 us (2%)
    pallas_call x1, Pallas kernels, fused(): pl.pallas_call(functools.partial(exchange_kernel, ep, tp, cap), out_shape...  57.9 us
    pallas_call x1, Pallas kernels, fused(): pl.pallas_call(weight_kernel, grid=(tp,), out_shape=(jax.ShapeDtypeStruct...  10.4 us

commit v1 on v0

v1 whole, which is shorter than its diff:
```python
import functools

import jax
import jax.numpy as jnp
from jax import lax
from jax.experimental import pallas as pl
from jax.experimental.pallas import tpu as pltpu
from jax.sharding import PartitionSpec as P

MESH = pl.DeviceIdType.MESH
BF16 = jnp.bfloat16
F32 = jnp.float32
MIB = 1024 * 1024


def dot_nn(a, b):
    return lax.dot_general(a, b, (((1,), (0,)), ((), ())), preferred_element_type=F32)


def flip(t, bit):
    return t + bit - 2 * bit * lax.rem(lax.div(t, bit), 2)


def partner(t, mask):
    bit = 1
    while bit <= mask:
        if mask & bit:
            t = flip(t, bit)
        bit *= 2
    return t


def exchange_kernel(
    ep, tp, cap,
    tok_ref, og_ref, routes_ref, gates_ref, wg_hbm, wu_hbm, wd_hbm,
    tg_ref, gg_ref, ggo, ugo, dgo,
    wg, wu, wd, wgt, wut, wdt, sent, big, comb_ref, pick_ref,
    hid, gp, up, hid_t, gp_t, up_t, dcol,
    psib, rsib, own_sum, mine, pown, rown, tsum, back, dsend, drecv, dsum, dback,
    wsem,
    zs, zr, ns, nr, ds_, dr, ss, sr,
    bss, bsr, rs, rr, zbs, zbr, dts, dtr, dzs, dzr,
):
    me_e = lax.axis_index("ep")
    me_t = lax.axis_index("tp")
    core = lax.rem(me_t, 2)
    sib = flip(me_t, 1)
    nbr = (flip(me_t, 2), flip(me_t, 4))
    diag = flip(nbr[0], 4)
    slots = ep * cap
    tok_dev, dw = tok_ref.shape
    fw, model = wg.shape

    def rdma(src, dst, s_sem, r_sem, e, t):
        return pltpu.make_async_remote_copy(
            src_ref=src, dst_ref=dst, send_sem=s_sem, recv_sem=r_sem,
            device_id={"ep": e, "tp": t}, device_id_type=MESH,
        )

    loads = [
        pltpu.make_async_copy(src.at[0], dst, wsem.at[i])
        for i, (src, dst) in enumerate(((wg_hbm, wg), (wu_hbm, wu), (wd_hbm, wd)))
    ]
    for load in loads:
        load.start()

    barrier = pltpu.get_barrier_semaphore()
    for r in range(1, ep):
        pl.semaphore_signal(
            barrier, inc=1, device_id={"ep": partner(me_e, r), "tp": me_t}, device_id_type=MESH)
    for r in range(1, tp):
        pl.semaphore_signal(
            barrier, inc=1, device_id={"ep": me_e, "tp": partner(me_t, r)}, device_id_type=MESH)

    expert = [routes_ref[k : k + 1, :] for k in range(2)]
    place = [jnp.zeros((1, tok_dev), F32) for _ in range(2)]
    for k in range(2):
        for i in range(ep):
            place[k] = jnp.where(expert[k] == partner(me_e, i), float(i), place[k])
    group = lax.broadcasted_iota(jnp.int32, (16, tok_dev), 0).astype(F32)
    oh = [jnp.where(place[k] == group, 1.0, 0.0) for k in range(2)]
    row_id = lax.broadcasted_iota(jnp.int32, (tok_dev, tok_dev), 0)
    col_id = lax.broadcasted_iota(jnp.int32, (tok_dev, tok_dev), 1)
    above = jnp.where(row_id < col_id, 1.0, 0.0).astype(BF16)
    before = dot_nn((oh[0] + oh[1]).astype(BF16), above)
    rank = [
        jnp.sum(before * oh[0], axis=0, keepdims=True),
        jnp.sum((before + oh[0]) * oh[1], axis=0, keepdims=True),
    ]
    slot_id = lax.broadcasted_iota(jnp.int32, (slots, tok_dev), 0).astype(F32)
    slot_gate = jnp.zeros((slots, 1), F32)
    both = jnp.zeros((slots, tok_dev), F32)
    for k in range(2):
        pick = jnp.where(place[k] * float(cap) + rank[k] == slot_id, 1.0, 0.0)
        pick_ref[k] = pick
        both = both + pick
        slot_gate = slot_gate + jnp.sum(pick * gates_ref[k : k + 1, :], axis=1, keepdims=True)
    select = both.astype(BF16)
    sent[:, 0:dw] = dot_nn(select, tok_ref[...]).astype(BF16)
    sent[:, dw : 2 * dw] = (slot_gate * dot_nn(select, og_ref[...])).astype(BF16)
    big[me_t, 0:cap, :] = sent[0:cap, :]

    pl.semaphore_wait(barrier, ep - 1 + tp - 1)

    sends = []

    def start(copy):
        copy.start()
        sends.append(copy)
        return copy

    def rows_of(i):
        return pl.ds(i * cap, cap)

    halves = (pl.ds(0, dw), pl.ds(dw, dw))
    z_copy, n_copy, d_copy, s_copy = {}, {}, {}, {}

    for i in range(1, ep):
        z_copy[i] = start(rdma(
            sent.at[rows_of(i)], big.at[me_t, rows_of(i)], zs.at[i], zr.at[i], partner(me_e, i), me_t))

    def chunk(i, t):
        return big.at[t, rows_of(i)]

    def half(i, t, h):
        return big.at[t, rows_of(i), halves[h]]

    def to_sibling(i, kind, t):
        s_copy[i, kind] = start(rdma(
            chunk(i, t), chunk(i, t), ss.at[i * 4 + kind], sr.at[i * 4 + kind], me_e, sib))

    def stage_a(i):
        if i:
            z_copy[i].wait_recv()
        for d in range(2):
            n_copy[i, d] = start(rdma(
                chunk(i, me_t), chunk(i, me_t), ns.at[i * 2 + d], nr.at[i * 2 + d], me_e, nbr[d]))
        to_sibling(i, 0, me_t)

    def stage_b(i):
        for d in range(2):
            n_copy[i, d].wait_recv()
            d_copy[i, d] = start(rdma(
                half(i, nbr[d], d), half(i, nbr[d], d), ds_.at[i * 2 + d], dr.at[i * 2 + d], me_e, nbr[1 - d]))
            to_sibling(i, 1 + d, nbr[d])

    def stage_c(i):
        for d in range(2):
            d_copy[i, d].wait_recv()
        to_sibling(i, 3, diag)

    def settle(i):
        for kind in range(4):
            s_copy[i, kind].wait_recv()

    def turn(w, wt):
        @pl.loop(0, tp)
        def _(j):
            part = pl.ds(pl.multiple_of(j * dw, dw), dw)
            wt[part, :] = w[:, part].T

    lane = lax.broadcasted_iota(jnp.int32, (cap, 128), 1)

    def forward(i):
        at = rows_of(i)

        def product(h, wt):
            total = dot_nn(big[0, at, halves[h]], wt[0:dw, :])
            for j in range(1, tp):
                total = total + dot_nn(big[j, at, halves[h]], wt[j * dw : (j + 1) * dw, :])
            return total

        g, u, h = product(0, wgt), product(0, wut), product(1, wdt)
        sig = jax.nn.sigmoid(g)
        act = g * sig
        hidden = (act * u).astype(BF16)
        hid[at, :] = hidden
        gp[at, :] = (h * u * sig * (1.0 + g * (1.0 - sig))).astype(BF16)
        up[at, :] = (h * act).astype(BF16)
        dots = jnp.sum(hidden.astype(F32) * h, axis=1, keepdims=True)
        dcol[0:cap, :] = jnp.where(lane == i, dots, dcol[0:cap, :])

    chips = (diag, nbr[0], nbr[1], me_t)
    b_copy, r_copy = {}, {}

    def pieces(i):
        at = rows_of(i)
        for q in range(4):
            wide = pl.ds(pl.multiple_of(lax.div(chips[q], 2) * (2 * dw), 2 * dw), 2 * dw)
            both = dot_nn(gp[at, :], wg[:, wide]) + dot_nn(up[at, :], wu[:, wide])
            low, high = both[:, 0:dw], both[:, dw : 2 * dw]
            psib[i, q] = jnp.where(core == 0, high, low).astype(BF16)
            own = jnp.where(core == 0, low, high)
            if q < 3:
                own_sum[i, q] = own
            else:
                mine[i] = own
            b_copy[i, q] = start(rdma(
                psib.at[i, q], rsib.at[i, q], bss.at[i * 4 + q], bsr.at[i * 4 + q], me_e, sib))

    def spread(i):
        for q in range(3):
            b_copy[i, q].wait_recv()
            pown[i, q] = (own_sum[i, q] + rsib[i, q].astype(F32)).astype(BF16)
            r_copy[i, q] = start(rdma(
                pown.at[i, q], rown.at[i, q], rs.at[i * 3 + q], rr.at[i * 3 + q], me_e, chips[q]))

    zb_copy = []

    def collect(i):
        b_copy[i, 3].wait_recv()
        total = mine[i] + rsib[i, 3].astype(F32)
        for q in range(3):
            r_copy[i, q].wait_recv()
            total = total + rown[i, q].astype(F32)
        if i:
            tsum[rows_of(i), :] = total.astype(BF16)
            zb_copy.append(start(rdma(
                tsum.at[rows_of(i)], back.at[rows_of(i)], zbs.at[i], zbr.at[i], partner(me_e, i), me_t)))
        else:
            back[rows_of(i), :] = total.astype(BF16)

    t_copy, dz_copy = [], []

    def send_dots():
        dsend[...] = dcol[...].T[0:8, :]
        for r in range(1, tp):
            t_copy.append(start(rdma(
                dsend, drecv.at[r - 1], dts.at[r - 1], dtr.at[r - 1], me_e, partner(me_t, r))))

    def return_dots():
        dots = dsend[...]
        for r in range(1, tp):
            t_copy[r - 1].wait_recv()
            dots = dots + drecv[r - 1]
        dsum[...] = dots
        for i in range(1, ep):
            dz_copy.append(start(rdma(
                dsum, dback.at[i], dzs.at[i], dzr.at[i], partner(me_e, i), me_t)))
        dback[0] = dots

    def weight_grad(rows_t, h, out):
        @pl.loop(0, tp)
        def _(j):
            part = pl.ds(pl.multiple_of(j * dw, dw), dw)
            out[:, part] = dot_nn(rows_t[...], big[j, :, halves[h]]).astype(BF16)

    dcol[...] = jnp.zeros_like(dcol)
    comb_ref[...] = both.T.astype(BF16)
    stage_a(0)
    loads[0].wait()
    turn(wg, wgt)
    loads[1].wait()
    turn(wu, wut)
    loads[2].wait()
    turn(wd, wdt)
    stage_b(0)
    stage_a(1)
    stage_c(0)
    if ep > 2:
        stage_a(2)
    settle(0)
    forward(0)
    stage_b(1)
    pieces(0)
    if ep > 2:
        stage_a(3)
        stage_b(2)
    stage_c(1)
    spread(0)
    settle(1)
    forward(1)
    if ep > 2:
        stage_b(3)
        pieces(1)
        stage_c(2)
        settle(2)
        forward(2)
        spread(1)
        collect(0)
        pieces(2)
        stage_c(3)
        spread(2)
        settle(3)
        forward(3)
        collect(1)
        send_dots()
        pieces(3)
        collect(2)
        hid_t[...] = hid[...].T
        gp_t[...] = gp[...].T
        up_t[...] = up[...].T
        spread(3)
        return_dots()
    else:
        send_dots()
        pieces(1)
        collect(0)
        hid_t[...] = hid[...].T
        gp_t[...] = gp[...].T
        up_t[...] = up[...].T
        spread(1)
        return_dots()
    weight_grad(gp_t, 0, ggo)
    collect(ep - 1)
    weight_grad(up_t, 0, ugo)
    weight_grad(hid_t, 1, dgo)

    for copy in dz_copy:
        copy.wait_recv()
    share = tok_dev // tp
    own_row = lax.broadcasted_iota(jnp.int32, (tok_dev, share), 0)
    own_col = lax.broadcasted_iota(jnp.int32, (tok_dev, share), 1) + me_t * share
    own_pick = jnp.where(own_row == own_col, 1.0, 0.0)
    tile_row = lax.broadcasted_iota(jnp.int32, (8, 128), 0)
    held = jnp.zeros((8, 128), F32)
    for i in range(ep):
        held = jnp.where(tile_row == i, dback[i], held)
    held = jnp.concatenate([held, jnp.zeros((120, 128), F32)], axis=0).T
    grads = []
    for k in range(2):
        total = jnp.zeros((1, tok_dev), F32)
        for i in range(ep):
            total = total + jnp.sum(
                held[0:cap, i : i + 1] * pick_ref[k, i * cap : (i + 1) * cap, :], axis=0, keepdims=True)
        grads.append(total / gates_ref[k : k + 1, :])
    shares = jnp.concatenate([*grads, jnp.zeros((6, tok_dev), F32)], axis=0)
    gg_ref[...] = jnp.dot(shares, own_pick, precision=lax.Precision.HIGHEST, preferred_element_type=F32)[0:2, :]

    for copy in zb_copy:
        copy.wait_recv()
    tg_ref[...] = dot_nn(comb_ref[...], back[...]).astype(BF16)
    for copy in sends:
        copy.wait_send()


def store_kernel(tg_ref, gg_ref, gw_ref, uw_ref, dw_ref, tg_out, gg_out, gw_out, uw_out, dw_out, sem):
    copies = [
        pltpu.make_async_copy(src, dst, sem.at[k])
        for k, (src, dst) in enumerate((
            (gw_ref, gw_out.at[0]), (uw_ref, uw_out.at[0]), (dw_ref, dw_out.at[0]),
            (tg_ref, tg_out), (gg_ref, gg_out)))
    ]
    for copy in copies:
        copy.start()
    for copy in copies:
        copy.wait()


def fused(tokens, out_grad, routes, gates, gate_weight, up_weight, down_weight):
    tok_dev, top_k = routes.shape
    ep = lax.axis_size("ep")
    tp = lax.axis_size("tp")
    cap = (3 * tok_dev + ep - 1) // ep
    slots = ep * cap
    dw = tokens.shape[1]
    model = gate_weight.shape[1]
    fw = gate_weight.shape[2]
    share = tok_dev // tp
    vmem = pl.BlockSpec(memory_space=pltpu.VMEM)
    any_ = pl.BlockSpec(memory_space=pl.ANY)
    dma = lambda n: pltpu.SemaphoreType.DMA((n,))
    flops = 16 * slots * model * fw
    small = (((tok_dev, dw), BF16), ((top_k, share), F32))
    grads = (((fw, model), BF16),) * 3
    results = pl.pallas_call(
        functools.partial(exchange_kernel, ep, tp, cap),
        out_shape=tuple(pltpu.VMEM(*leaf) for leaf in small + grads),
        in_specs=[vmem] * 4 + [any_] * 3,
        out_specs=[vmem] * 5,
        scratch_shapes=[
            pltpu.VMEM((fw, model), BF16),
            pltpu.VMEM((fw, model), BF16),
            pltpu.VMEM((fw, model), BF16),
            pltpu.VMEM((model, fw), BF16),
            pltpu.VMEM((model, fw), BF16),
            pltpu.VMEM((model, fw), BF16),
            pltpu.VMEM((slots, 2 * dw), BF16),
            pltpu.VMEM((tp, slots, 2 * dw), BF16),
            pltpu.VMEM((tok_dev, slots), BF16),
            pltpu.VMEM((2, slots, tok_dev), F32),
            pltpu.VMEM((slots, fw), BF16),
            pltpu.VMEM((slots, fw), BF16),
            pltpu.VMEM((slots, fw), BF16),
            pltpu.VMEM((fw, slots), BF16),
            pltpu.VMEM((fw, slots), BF16),
            pltpu.VMEM((fw, slots), BF16),
            pltpu.VMEM((128, 128), F32),
            pltpu.VMEM((ep, 4, cap, dw), BF16),
            pltpu.VMEM((ep, 4, cap, dw), BF16),
            pltpu.VMEM((ep, 3, cap, dw), F32),
            pltpu.VMEM((ep, cap, dw), F32),
            pltpu.VMEM((ep, 3, cap, dw), BF16),
            pltpu.VMEM((ep, 3, cap, dw), BF16),
            pltpu.VMEM((slots, dw), BF16),
            pltpu.VMEM((slots, dw), BF16),
            pltpu.VMEM((8, 128), F32),
            pltpu.VMEM((tp - 1, 8, 128), F32),
            pltpu.VMEM((8, 128), F32),
            pltpu.VMEM((ep, 8, 128), F32),
            dma(3),
            dma(ep), dma(ep), dma(2 * ep), dma(2 * ep), dma(2 * ep), dma(2 * ep),
            dma(4 * ep), dma(4 * ep),
            dma(4 * ep), dma(4 * ep), dma(3 * ep), dma(3 * ep), dma(ep), dma(ep),
            dma(tp), dma(tp), dma(ep), dma(ep),
        ],
        compiler_params=pltpu.CompilerParams(
            collective_id=0, has_side_effects=True, vmem_limit_bytes=46 * MIB),
        cost_estimate=pl.CostEstimate(flops=flops, bytes_accessed=6 * model * fw, transcendentals=0),
    )(tokens, out_grad, routes.T, gates.T, jnp.swapaxes(gate_weight, 1, 2),
      jnp.swapaxes(up_weight, 1, 2), down_weight)
    held = [pltpu.with_memory_space_constraint(r, pltpu.VMEM) for r in results]
    tokens_grad, gates_grad, gate_grad, up_grad, down_grad = pl.pallas_call(
        store_kernel,
        out_shape=tuple(jax.ShapeDtypeStruct(*leaf) for leaf in small)
        + tuple(jax.ShapeDtypeStruct((1, *shape), dtype) for shape, dtype in grads),
        in_specs=[vmem] * 5,
        out_specs=[any_] * 5,
        scratch_shapes=[dma(5)],
        compiler_params=pltpu.CompilerParams(vmem_limit_bytes=16 * MIB),
        cost_estimate=pl.CostEstimate(flops=slots * fw, bytes_accessed=6 * model * fw, transcendentals=0),
    )(*held)
    return (tokens_grad, gates_grad.T, jnp.swapaxes(gate_grad, 1, 2), jnp.swapaxes(up_grad, 1, 2), down_grad)


def fits_fused(ep, tp, tokens, routes, gate_weight):
    cap = (3 * routes.shape[0] + ep - 1) // ep
    return (
        tp == 8 and ep in (2, 4) and cap % 16 == 0 and cap <= 128
        and tokens.shape[1] % 128 == 0 and routes.shape[1] == 2
        and routes.shape[0] == 128
        and gate_weight.shape[2] % 16 == 0
    )


def expert_grads(rows, cotan, w_gate, w_up, w_down):
    pre_gate = jnp.dot(rows, w_gate, preferred_element_type=jnp.float32)
    pre_up = jnp.dot(rows, w_up, preferred_element_type=jnp.float32)
    activated = jax.nn.silu(pre_gate)
    hidden = (activated * pre_up).astype(jnp.bfloat16)
    hid_grad = jnp.dot(cotan, w_down.T, preferred_element_type=jnp.float32)
    sigmoid_gate = jax.nn.sigmoid(pre_gate)
    gate_part = (hid_grad * pre_up * sigmoid_gate * (1.0 + pre_gate * (1.0 - sigmoid_gate))).astype(
        jnp.bfloat16
    )
    up_part = (hid_grad * activated).astype(jnp.bfloat16)
    slot_dots = jnp.sum(hidden.astype(jnp.float32) * hid_grad, axis=1)
    down_grad = jnp.dot(hidden.T, cotan, preferred_element_type=jnp.float32).astype(jnp.bfloat16)
    gate_grad = jnp.dot(rows.T, gate_part, preferred_element_type=jnp.float32).astype(jnp.bfloat16)
    up_grad = jnp.dot(rows.T, up_part, preferred_element_type=jnp.float32).astype(jnp.bfloat16)
    return (gate_part, up_part, slot_dots, gate_grad, up_grad, down_grad)


def on_device(tokens, out_grad, routes, gates, gate_weight, up_weight, down_weight):
    tok_dev, top_k = routes.shape
    ep_size = lax.axis_size("ep")
    tp_size = lax.axis_size("tp")
    if fits_fused(ep_size, tp_size, tokens, routes, gate_weight):
        return fused(tokens, out_grad, routes, gates, gate_weight, up_weight, down_weight)
    capacity = (3 * tok_dev + ep_size - 1) // ep_size
    buffer_rows = ep_size * capacity
    slice_width = tokens.shape[1]
    flat_expert = routes.reshape(-1)
    onehot = (flat_expert[:, None] == jnp.arange(ep_size, dtype=jnp.int32)[None, :]).astype(
        jnp.int32
    )
    slot_rank = jnp.sum((jnp.cumsum(onehot, axis=0) - onehot) * onehot, axis=1)
    slot_dest = flat_expert * capacity + slot_rank
    placed = jnp.arange(buffer_rows, dtype=jnp.int32)[:, None] == slot_dest[None, :]
    placed_float = placed.astype(jnp.float32)
    select = jnp.any(placed.reshape(buffer_rows, tok_dev, top_k), axis=2).astype(jnp.bfloat16)
    slot_gate = jnp.dot(placed_float, gates.reshape(-1), precision=lax.Precision.HIGHEST)
    sent_rows = jnp.dot(select, tokens, preferred_element_type=jnp.float32).astype(jnp.bfloat16)
    cotan_rows = jnp.dot(select, out_grad, preferred_element_type=jnp.float32)
    sent_cotan = (slot_gate[:, None] * cotan_rows).astype(jnp.bfloat16)
    recv_rows, recv_cotan = (
        lax.all_to_all(
            sent_rows.reshape(ep_size, capacity, slice_width),
            "ep",
            split_axis=0,
            concat_axis=0,
            tiled=True,
        ),
        lax.all_to_all(
            sent_cotan.reshape(ep_size, capacity, slice_width),
            "ep",
            split_axis=0,
            concat_axis=0,
            tiled=True,
        ),
    )
    whole_rows, whole_cotan = (
        lax.all_gather(recv_rows, "tp", axis=2, tiled=True),
        lax.all_gather(recv_cotan, "tp", axis=2, tiled=True),
    )
    model_width = whole_rows.shape[2]
    rows = whole_rows.reshape(buffer_rows, model_width)
    cotan = whole_cotan.reshape(buffer_rows, model_width)
    w_gate = gate_weight[0]
    w_up = up_weight[0]
    gate_part, up_part, slot_dots, gate_grad, up_grad, down_grad = expert_grads(
        rows, cotan, w_gate, w_up, down_weight[0]
    )
    partial_value = jnp.dot(gate_part, w_gate.T, preferred_element_type=jnp.float32)
    partial_value = (
        partial_value + jnp.dot(up_part, w_up.T, preferred_element_type=jnp.float32)
    ).astype(jnp.bfloat16)
    share = tok_dev // tp_size
    start = lax.axis_index("tp") * share
    summed = lax.psum(slot_dots, "tp")
    row_sums = lax.psum_scatter(
        partial_value.reshape(ep_size, capacity, model_width), "tp", scatter_dimension=2, tiled=True
    ).astype(jnp.float32)
    back_rows, back_dots = (
        lax.all_to_all(
            row_sums.astype(jnp.bfloat16), "ep", split_axis=0, concat_axis=0, tiled=True
        ).astype(row_sums.dtype),
        lax.all_to_all(
            summed.reshape(ep_size, capacity).astype(jnp.bfloat16),
            "ep",
            split_axis=0,
            concat_axis=0,
            tiled=True,
        ).astype(jnp.float32),
    )
    slot_rows = back_rows.reshape(buffer_rows, slice_width)[slot_dest]
    tokens_grad = jnp.sum(slot_rows.reshape(tok_dev, top_k, slice_width), axis=1).astype(
        jnp.bfloat16
    )
    token_dots = back_dots.reshape(buffer_rows)[slot_dest].reshape(tok_dev, top_k)
    own_dots = lax.dynamic_slice_in_dim(token_dots, start, share, 0)
    own_gates = lax.dynamic_slice_in_dim(gates, start, share, 0)
    gates_grad = own_dots / own_gates
    return (tokens_grad, gates_grad, gate_grad[None], up_grad[None], down_grad[None])


def solution(mesh):
    placed = (
        P("ep", "tp"),
        P("ep", "tp"),
        P("ep", None),
        P("ep", None),
        P("ep", None, "tp"),
        P("ep", None, "tp"),
        P("ep", "tp", None),
    )
    return jax.shard_map(
        on_device,
        mesh=mesh,
        in_specs=placed,
        out_specs=(
            P("ep", "tp"),
            P(("ep", "tp"), None),
            P("ep", None, "tp"),
            P("ep", None, "tp"),
            P("ep", "tp", None),
        ),
        check_vma=False,
    )
```

time: 70.5 us -> 53 us (0.75)
  Pallas kernels: 68.3 us -> 52.2 us
  local copies, waits for them, and re-layouts: 1.2 us -> 0 us
    pallas_call x1, Pallas kernels: 57.9 us -> 48.7 us  [fused(): pl.pallas_call(functools.partial(exchange_kernel, ep, tp, cap), out_shape...]
    pallas_call x1, Pallas kernels: 10.4 us -> 3.53 us  [fused(): pl.pallas_call(store_kernel, out_shape=tuple((jax.ShapeDtypeStruct(*leaf)...]
    unnamed x6 -> x0, local copies, waits for them, and re-layouts: 1.2 us -> none
where the time goes in v1:
time: 53 us; the launch traced here: 52.8 us
  Pallas kernels  52.2 us (98%)
  between operations  0.64 us (1%)
    pallas_call x1, Pallas kernels, fused(): pl.pallas_call(functools.partial(exchange_kernel, ep, tp, cap), out_shape...  48.7 us
    pallas_call x1, Pallas kernels, fused(): pl.pallas_call(store_kernel, out_shape=tuple((jax.ShapeDtypeStruct(*leaf)...  3.53 us

profile of v1, /device:TPU:0, one launch (start us, length us, event | category | flops | bytes accessed | tf_op | source)
XLA Modules:
  0.0 52.8 jit_solution(2375687469046049651)
XLA Ops:
  0.6 48.7 %shard_map.110 = (bf16[128,256]{1,0:T(8,128)(2,1)S(1)}, f32[2,16]{1,0:T(2,128)S(1)}, bf16[704,2048]{1,0:T(8,128)(2,1)S(1)}, bf16[704,2048]{1,0:T(8,128)(2,1)S(1)}, bf16[704,2048]{1,0:T(8,128)(2,1)S(1)}) custom-call(bf16[128,256]{1,0:T(8,128)(2,1)} %tok_ref.1, bf16[128,256]{1,0:T(8,128)(2,1)} %og_ref.1, s32[2,128]{1,0:T(2,128)} %bitcast.11, ...), custom_call_target="tpu_custom_call" | custom-call | flops 8858370048 | bytes 8650752 | tf_op jit(solution)/shard_map/pallas_call | solution.py:366
  49.3 3.5 %shard_map.111 = (bf16[128,256]{1,0:T(8,128)(2,1)}, f32[2,16]{1,0:T(2,128)}, bf16[1,704,2048]{2,1,0:T(8,128)(2,1)}, bf16[1,704,2048]{2,1,0:T(8,128)(2,1)}, bf16[1,704,2048]{2,1,0:T(8,128)(2,1)}) custom-call(bf16[128,256]{1,0:T(8,128)(2,1)S(1)} %get-tuple-element.15.tg_ref, f32[2,16]{1,0:T(2,128)S(1)} %get-tuple-element.16.gg_ref, ...), custom_call_target="tpu_custom_call" | custom-call | flops 270336 | bytes 8650752 | tf_op jit(solution)/shard_map/pallas_call | solution.py:413

commit v2 on v1

--- a/solution.py
+++ b/solution.py
@@ -35,11 +35,9 @@
     tok_ref, og_ref, routes_ref, gates_ref, wg_hbm, wu_hbm, wd_hbm,
     tg_ref, gg_ref, ggo, ugo, dgo,
     wg, wu, wd, wgt, wut, wdt, sent, big, comb_ref, pick_ref,
-    hid, gp, up, hid_t, gp_t, up_t, dcol,
-    psib, rsib, own_sum, mine, pown, rown, tsum, back, dsend, drecv, dsum, dback,
-    wsem,
-    zs, zr, ns, nr, ds_, dr, ss, sr,
-    bss, bsr, rs, rr, zbs, zbr, dts, dtr, dzs, dzr,
+    pg, pu, hid, gp, up, hid_t, gp_t, up_t, dcol,
+    psib, rsib, own_sum, pown, rown, tsum, back, dsend, drecv, dsum, dback,
+    wsem, out_sem, zr, nr, dr, sr, br, rr, zbr, dtr, dzr,
 ):
     me_e = lax.axis_index("ep")
     me_t = lax.axis_index("tp")
@@ -51,11 +49,14 @@
     tok_dev, dw = tok_ref.shape
     fw, model = wg.shape
 
-    def rdma(src, dst, s_sem, r_sem, e, t):
+    def rdma(src, dst, sem, e, t):
         return pltpu.make_async_remote_copy(
-            src_ref=src, dst_ref=dst, send_sem=s_sem, recv_sem=r_sem,
+            src_ref=src, dst_ref=dst, send_sem=out_sem.at[0], recv_sem=sem,
             device_id={"ep": e, "tp": t}, device_id_type=MESH,
         )
+
+    def arrived(ref, sem):
+        rdma(ref, ref, sem, me_e, sib).wait_recv()
 
     loads = [
         pltpu.make_async_copy(src.at[0], dst, wsem.at[i])
@@ -104,20 +105,16 @@
 
     sends = []
 
-    def start(copy):
+    def send(src, dst, sem, e, t):
+        copy = rdma(src, dst, sem, e, t)
         copy.start()
         sends.append(copy)
-        return copy
 
     def rows_of(i):
         return pl.ds(i * cap, cap)
 
     halves = (pl.ds(0, dw), pl.ds(dw, dw))
-    z_copy, n_copy, d_copy, s_copy = {}, {}, {}, {}
-
-    for i in range(1, ep):
-        z_copy[i] = start(rdma(
-            sent.at[rows_of(i)], big.at[me_t, rows_of(i)], zs.at[i], zr.at[i], partner(me_e, i), me_t))
+    direct = ()
 
     def chunk(i, t):
         return big.at[t, rows_of(i)]
@@ -125,33 +122,35 @@
     def half(i, t, h):
         return big.at[t, rows_of(i), halves[h]]
 
-    def to_sibling(i, kind, t):
-        s_copy[i, kind] = start(rdma(
-            chunk(i, t), chunk(i, t), ss.at[i * 4 + kind], sr.at[i * 4 + kind], me_e, sib))
+    def to_sibling(i, t):
+        send(chunk(i, t), chunk(i, t), sr.at[i], me_e, sib)
+
+    def send_z(i):
+        return rdma(sent.at[rows_of(i)], big.at[me_t, rows_of(i)], zr.at[i], partner(me_e, i), me_t)
 
     def stage_a(i):
         if i:
-            z_copy[i].wait_recv()
+            arrived(chunk(i, me_t), zr.at[i])
         for d in range(2):
-            n_copy[i, d] = start(rdma(
-                chunk(i, me_t), chunk(i, me_t), ns.at[i * 2 + d], nr.at[i * 2 + d], me_e, nbr[d]))
-        to_sibling(i, 0, me_t)
+            send(chunk(i, me_t), chunk(i, me_t), nr.at[2 * i + d], me_e, nbr[d])
+        if i in direct:
+            send(chunk(i, me_t), chunk(i, me_t), dr.at[i], me_e, diag)
+        to_sibling(i, me_t)
 
     def stage_b(i):
         for d in range(2):
-            n_copy[i, d].wait_recv()
-            d_copy[i, d] = start(rdma(
-                half(i, nbr[d], d), half(i, nbr[d], d), ds_.at[i * 2 + d], dr.at[i * 2 + d], me_e, nbr[1 - d]))
-            to_sibling(i, 1 + d, nbr[d])
+            arrived(chunk(i, nbr[d]), nr.at[2 * i + d])
+            if i not in direct:
+                send(half(i, nbr[d], d), half(i, nbr[d], d), dr.at[i], me_e, nbr[1 - d])
+        for d in range(2):
+            to_sibling(i, nbr[d])
 
     def stage_c(i):
-        for d in range(2):
-            d_copy[i, d].wait_recv()
-        to_sibling(i, 3, diag)
+        arrived(chunk(i, diag), dr.at[i])
+        to_sibling(i, diag)
 
     def settle(i):
-        for kind in range(4):
-            s_copy[i, kind].wait_recv()
+        arrived(big.at[pl.ds(0, 4), rows_of(i)], sr.at[i])
 
     def turn(w, wt):
         @pl.loop(0, tp)
@@ -161,16 +160,20 @@
 
     lane = lax.broadcasted_iota(jnp.int32, (cap, 128), 1)
 
-    def forward(i):
+    def product(i, h, wt):
         at = rows_of(i)
-
-        def product(h, wt):
-            total = dot_nn(big[0, at, halves[h]], wt[0:dw, :])
-            for j in range(1, tp):
-                total = total + dot_nn(big[j, at, halves[h]], wt[j * dw : (j + 1) * dw, :])
-            return total
-
-        g, u, h = product(0, wgt), product(0, wut), product(1, wdt)
+        total = dot_nn(big[0, at, halves[h]], wt[0:dw, :])
+        for j in range(1, tp):
+            total = total + dot_nn(big[j, at, halves[h]], wt[j * dw : (j + 1) * dw, :])
+        return total
+
+    def forward_x(i):
+        pg[...] = product(i, 0, wgt)
+        pu[...] = product(i, 0, wut)
+
+    def forward_c(i):
+        at = rows_of(i)
+        g, u, h = pg[...], pu[...], product(i, 1, wdt)
         sig = jax.nn.sigmoid(g)
         act = g * sig
         hidden = (act * u).astype(BF16)
@@ -181,7 +184,6 @@
         dcol[0:cap, :] = jnp.where(lane == i, dots, dcol[0:cap, :])
 
     chips = (diag, nbr[0], nbr[1], me_t)
-    b_copy, r_copy = {}, {}
 
     def pieces(i):
         at = rows_of(i)
@@ -190,124 +192,126 @@
             both = dot_nn(gp[at, :], wg[:, wide]) + dot_nn(up[at, :], wu[:, wide])
             low, high = both[:, 0:dw], both[:, dw : 2 * dw]
             psib[i, q] = jnp.where(core == 0, high, low).astype(BF16)
-            own = jnp.where(core == 0, low, high)
-            if q < 3:
-                own_sum[i, q] = own
-            else:
-                mine[i] = own
-            b_copy[i, q] = start(rdma(
-                psib.at[i, q], rsib.at[i, q], bss.at[i * 4 + q], bsr.at[i * 4 + q], me_e, sib))
+            own_sum[i, q] = jnp.where(core == 0, low, high)
+        send(psib.at[i], rsib.at[i], br.at[i], me_e, sib)
 
     def spread(i):
+        arrived(rsib.at[i], br.at[i])
         for q in range(3):
-            b_copy[i, q].wait_recv()
             pown[i, q] = (own_sum[i, q] + rsib[i, q].astype(F32)).astype(BF16)
-            r_copy[i, q] = start(rdma(
-                pown.at[i, q], rown.at[i, q], rs.at[i * 3 + q], rr.at[i * 3 + q], me_e, chips[q]))
-
-    zb_copy = []
+        for q in range(3):
+            send(pown.at[i, q], rown.at[i, q], rr.at[i], me_e, chips[q])
 
     def collect(i):
-        b_copy[i, 3].wait_recv()
-        total = mine[i] + rsib[i, 3].astype(F32)
+        arrived(rown.at[i], rr.at[i])
+        total = own_sum[i, 3] + rsib[i, 3].astype(F32)
         for q in range(3):
-            r_copy[i, q].wait_recv()
             total = total + rown[i, q].astype(F32)
         if i:
             tsum[rows_of(i), :] = total.astype(BF16)
-            zb_copy.append(start(rdma(
-                tsum.at[rows_of(i)], back.at[rows_of(i)], zbs.at[i], zbr.at[i], partner(me_e, i), me_t)))
+            send(tsum.at[rows_of(i)], back.at[rows_of(i)], zbr.at[0], partner(me_e, i), me_t)
         else:
             back[rows_of(i), :] = total.astype(BF16)
-
-    t_copy, dz_copy = [], []
 
     def send_dots():
         dsend[...] = dcol[...].T[0:8, :]
         for r in range(1, tp):
-            t_copy.append(start(rdma(
-                dsend, drecv.at[r - 1], dts.at[r - 1], dtr.at[r - 1], me_e, partner(me_t, r))))
+            send(dsend, drecv.at[r - 1], dtr.at[0], me_e, partner(me_t, r))
 
     def return_dots():
+        arrived(drecv, dtr.at[0])
         dots = dsend[...]
         for r in range(1, tp):
-            t_copy[r - 1].wait_recv()
             dots = dots + drecv[r - 1]
         dsum[...] = dots
         for i in range(1, ep):
-            dz_copy.append(start(rdma(
-                dsum, dback.at[i], dzs.at[i], dzr.at[i], partner(me_e, i), me_t)))
+            send(dsum, dback.at[i], dzr.at[0], partner(me_e, i), me_t)
         dback[0] = dots
 
-    def weight_grad(rows_t, h, out):
-        @pl.loop(0, tp)
-        def _(j):
-            part = pl.ds(pl.multiple_of(j * dw, dw), dw)
-            out[:, part] = dot_nn(rows_t[...], big[j, :, halves[h]]).astype(BF16)
-
+    def weight_grad(rows_t, h, out, lo, hi):
+        for k in range(lo, hi):
+            out[:, k * dw : (k + 1) * dw] = dot_nn(rows_t[...], big[k, :, halves[h]]).astype(BF16)
+
+    def flats():
+        hid_t[...] = hid[...].T
+        gp_t[...] = gp[...].T
+        up_t[...] = up[...].T
+
+    z_order = (1, 3, 2) if ep == 4 else (1,)
+    z_sends = [send_z(i) for i in z_order]
+    sends.extend(z_sends)
+    for copy in z_sends:
+        copy.start()
+    stage_a(0)
     dcol[...] = jnp.zeros_like(dcol)
     comb_ref[...] = both.T.astype(BF16)
-    stage_a(0)
-    loads[0].wait()
-    turn(wg, wgt)
-    loads[1].wait()
-    turn(wu, wut)
-    loads[2].wait()
-    turn(wd, wdt)
+    for k, (w, wt) in enumerate(((wg, wgt), (wu, wut), (wd, wdt))):
+        loads[k].wait()
+        turn(w, wt)
     stage_b(0)
     stage_a(1)
     stage_c(0)
-    if ep > 2:
+    settle(0)
+    forward_x(0)
+    stage_b(1)
+    if ep == 4:
+        forward_c(0)
+        stage_a(3)
+        pieces(0)
         stage_a(2)
-    settle(0)
-    forward(0)
-    stage_b(1)
-    pieces(0)
-    if ep > 2:
-        stage_a(3)
+        stage_c(1)
+        settle(1)
+        forward_x(1)
+        stage_b(3)
+        forward_c(1)
         stage_b(2)
-    stage_c(1)
-    spread(0)
-    settle(1)
-    forward(1)
-    if ep > 2:
-        stage_b(3)
         pieces(1)
+        stage_c(3)
+        settle(3)
+        forward_x(3)
+        spread(1)
         stage_c(2)
+        forward_c(3)
+        pieces(3)
         settle(2)
-        forward(2)
-        spread(1)
-        collect(0)
-        pieces(2)
-        stage_c(3)
-        spread(2)
-        settle(3)
-        forward(3)
+        forward_x(2)
+        spread(3)
+        forward_c(2)
         collect(1)
         send_dots()
-        pieces(3)
+        pieces(2)
+        flats()
+        weight_grad(gp_t, 0, ggo, 0, 4)
+        spread(2)
+        collect(3)
+        return_dots()
+        spread(0)
+        weight_grad(gp_t, 0, ggo, 4, 8)
+        weight_grad(up_t, 0, ugo, 0, 8)
         collect(2)
-        hid_t[...] = hid[...].T
-        gp_t[...] = gp[...].T
-        up_t[...] = up[...].T
-        spread(3)
-        return_dots()
+        weight_grad(hid_t, 1, dgo, 0, 4)
+        collect(0)
+        weight_grad(hid_t, 1, dgo, 4, 8)
     else:
+        forward_c(0)
+        stage_c(1)
+        settle(1)
+        forward_x(1)
+        forward_c(1)
         send_dots()
         pieces(1)
+        pieces(0)
+        spread(1)
+        flats()
+        return_dots()
+        spread(0)
+        weight_grad(gp_t, 0, ggo, 0, 8)
+        weight_grad(up_t, 0, ugo, 0, 8)
+        collect(1)
         collect(0)
-        hid_t[...] = hid[...].T
-        gp_t[...] = gp[...].T
-        up_t[...] = up[...].T
-        spread(1)
-        return_dots()
-    weight_grad(gp_t, 0, ggo)
-    collect(ep - 1)
-    weight_grad(up_t, 0, ugo)
-    weight_grad(hid_t, 1, dgo)
-
-    for copy in dz_copy:
-        copy.wait_recv()
+        weight_grad(hid_t, 1, dgo, 0, 8)
+
+    arrived(dback.at[pl.ds(1, ep - 1)], dzr.at[0])
     share = tok_dev // tp
     own_row = lax.broadcasted_iota(jnp.int32, (tok_dev, share), 0)
     own_col = lax.broadcasted_iota(jnp.int32, (tok_dev, share), 1) + me_t * share
@@ -327,8 +331,7 @@
     shares = jnp.concatenate([*grads, jnp.zeros((6, tok_dev), F32)], axis=0)
     gg_ref[...] = jnp.dot(shares, own_pick, precision=lax.Precision.HIGHEST, preferred_element_type=F32)[0:2, :]
 
-    for copy in zb_copy:
-        copy.wait_recv()
+    arrived(back.at[pl.ds(cap, slots - cap)], zbr.at[0])
     tg_ref[...] = dot_nn(comb_ref[...], back[...]).astype(BF16)
     for copy in sends:
         copy.wait_send()
@@ -379,6 +382,8 @@
             pltpu.VMEM((tp, slots, 2 * dw), BF16),
             pltpu.VMEM((tok_dev, slots), BF16),
             pltpu.VMEM((2, slots, tok_dev), F32),
+            pltpu.VMEM((cap, fw), F32),
+            pltpu.VMEM((cap, fw), F32),
             pltpu.VMEM((slots, fw), BF16),
             pltpu.VMEM((slots, fw), BF16),
             pltpu.VMEM((slots, fw), BF16),
@@ -388,8 +393,7 @@
             pltpu.VMEM((128, 128), F32),
             pltpu.VMEM((ep, 4, cap, dw), BF16),
             pltpu.VMEM((ep, 4, cap, dw), BF16),
-            pltpu.VMEM((ep, 3, cap, dw), F32),
-            pltpu.VMEM((ep, cap, dw), F32),
+            pltpu.VMEM((ep, 4, cap, dw), F32),
             pltpu.VMEM((ep, 3, cap, dw), BF16),
             pltpu.VMEM((ep, 3, cap, dw), BF16),
             pltpu.VMEM((slots, dw), BF16),
@@ -398,11 +402,7 @@
             pltpu.VMEM((tp - 1, 8, 128), F32),
             pltpu.VMEM((8, 128), F32),
             pltpu.VMEM((ep, 8, 128), F32),
-            dma(3),
-            dma(ep), dma(ep), dma(2 * ep), dma(2 * ep), dma(2 * ep), dma(2 * ep),
-            dma(4 * ep), dma(4 * ep),
-            dma(4 * ep), dma(4 * ep), dma(3 * ep), dma(3 * ep), dma(ep), dma(ep),
-            dma(tp), dma(tp), dma(ep), dma(ep),
+            dma(3), dma(1), dma(ep), dma(2 * ep), dma(ep), dma(ep), dma(ep), dma(ep), dma(1), dma(1), dma(1),
         ],
         compiler_params=pltpu.CompilerParams(
             collective_id=0, has_side_effects=True, vmem_limit_bytes=46 * MIB),

time: 53 us -> 47.7 us (0.900)
  Pallas kernels: 52.2 us -> 46.7 us
    pallas_call x1, Pallas kernels: 48.7 us -> 43.2 us  [fused(): pl.pallas_call(functools.partial(exchange_kernel, ep, tp, cap), out_shape...]
where the time goes in v2:
time: 47.7 us; the launch traced here: 47.5 us
  Pallas kernels  46.7 us (98%)
  between operations  0.8 us (2%)
    pallas_call x1, Pallas kernels, fused(): pl.pallas_call(functools.partial(exchange_kernel, ep, tp, cap), out_shape...  43.2 us
    pallas_call x1, Pallas kernels, fused(): pl.pallas_call(store_kernel, out_shape=tuple((jax.ShapeDtypeStruct(*leaf)...  3.53 us

profile of v2, /device:TPU:0, one launch (start us, length us, event | category | flops | bytes accessed | tf_op | source)
XLA Modules:
  0.0 47.5 jit_solution(5438434925180090801)
XLA Ops:
  0.6 43.2 %shard_map.110 = (bf16[128,256]{1,0:T(8,128)(2,1)S(1)}, f32[2,16]{1,0:T(2,128)S(1)}, bf16[704,2048]{1,0:T(8,128)(2,1)S(1)}, bf16[704,2048]{1,0:T(8,128)(2,1)S(1)}, bf16[704,2048]{1,0:T(8,128)(2,1)S(1)}) custom-call(bf16[128,256]{1,0:T(8,128)(2,1)} %tok_ref.1, bf16[128,256]{1,0:T(8,128)(2,1)} %og_ref.1, s32[2,128]{1,0:T(2,128)} %bitcast.11, ...), custom_call_target="tpu_custom_call" | custom-call | flops 8858370048 | bytes 8650752 | tf_op jit(solution)/shard_map/pallas_call | solution.py:369
  43.8 3.5 %shard_map.111 = (bf16[128,256]{1,0:T(8,128)(2,1)}, f32[2,16]{1,0:T(2,128)}, bf16[1,704,2048]{2,1,0:T(8,128)(2,1)}, bf16[1,704,2048]{2,1,0:T(8,128)(2,1)}, bf16[1,704,2048]{2,1,0:T(8,128)(2,1)}) custom-call(bf16[128,256]{1,0:T(8,128)(2,1)S(1)} %get-tuple-element.15.tg_ref, f32[2,16]{1,0:T(2,128)S(1)} %get-tuple-element.16.gg_ref, ...), custom_call_target="tpu_custom_call" | custom-call | flops 270336 | bytes 8650752 | tf_op jit(solution)/shard_map/pallas_call | solution.py:413

commit v3 on v2

--- a/solution.py
+++ b/solution.py
@@ -32,12 +32,12 @@
 
 def exchange_kernel(
     ep, tp, cap,
-    tok_ref, og_ref, routes_ref, gates_ref, wg_hbm, wu_hbm, wd_hbm,
+    tok_hbm, og_hbm, routes_hbm, gates_hbm, wg_hbm, wu_hbm, wd_hbm,
     tg_ref, gg_ref, ggo, ugo, dgo,
-    wg, wu, wd, wgt, wut, wdt, sent, big, comb_ref, pick_ref,
-    pg, pu, hid, gp, up, hid_t, gp_t, up_t, dcol,
+    tok_ref, og_ref, routes_ref, gates_ref, wg, wu, wd, wgt, wut, wdt, sent, big, comb_ref, pick_ref,
+    pg, pu, ph, hid, gp, up, hid_t, gp_t, up_t, dcol,
     psib, rsib, own_sum, pown, rown, tsum, back, dsend, drecv, dsum, dback,
-    wsem, out_sem, zr, nr, dr, sr, br, rr, zbr, dtr, dzr,
+    isem, wsem, out_sem, zr, nr, dr, sr, br, rr, zbr, dtr, dzr,
 ):
     me_e = lax.axis_index("ep")
     me_t = lax.axis_index("tp")
@@ -58,13 +58,17 @@
     def arrived(ref, sem):
         rdma(ref, ref, sem, me_e, sib).wait_recv()
 
+    inputs = [
+        pltpu.make_async_copy(src, dst, isem.at[i])
+        for i, (src, dst) in enumerate((
+            (routes_hbm, routes_ref), (gates_hbm, gates_ref), (tok_hbm, tok_ref), (og_hbm, og_ref)))
+    ]
+    for load in inputs:
+        load.start()
     loads = [
         pltpu.make_async_copy(src.at[0], dst, wsem.at[i])
         for i, (src, dst) in enumerate(((wg_hbm, wg), (wu_hbm, wu), (wd_hbm, wd)))
     ]
-    for load in loads:
-        load.start()
-
     barrier = pltpu.get_barrier_semaphore()
     for r in range(1, ep):
         pl.semaphore_signal(
@@ -72,6 +76,11 @@
     for r in range(1, tp):
         pl.semaphore_signal(
             barrier, inc=1, device_id={"ep": me_e, "tp": partner(me_t, r)}, device_id_type=MESH)
+
+    for load in loads:
+        load.start()
+    for load in inputs:
+        load.wait()
 
     expert = [routes_ref[k : k + 1, :] for k in range(2)]
     place = [jnp.zeros((1, tok_dev), F32) for _ in range(2)]
@@ -114,7 +123,7 @@
         return pl.ds(i * cap, cap)
 
     halves = (pl.ds(0, dw), pl.ds(dw, dw))
-    direct = ()
+    direct = (1,)
 
     def chunk(i, t):
         return big.at[t, rows_of(i)]
@@ -122,8 +131,8 @@
     def half(i, t, h):
         return big.at[t, rows_of(i), halves[h]]
 
-    def to_sibling(i, t):
-        send(chunk(i, t), chunk(i, t), sr.at[i], me_e, sib)
+    def to_sibling(i, t, far=0):
+        send(chunk(i, t), chunk(i, t), sr.at[2 * i + far], me_e, sib)
 
     def send_z(i):
         return rdma(sent.at[rows_of(i)], big.at[me_t, rows_of(i)], zr.at[i], partner(me_e, i), me_t)
@@ -147,10 +156,13 @@
 
     def stage_c(i):
         arrived(chunk(i, diag), dr.at[i])
-        to_sibling(i, diag)
-
-    def settle(i):
-        arrived(big.at[pl.ds(0, 4), rows_of(i)], sr.at[i])
+        to_sibling(i, diag, 1)
+
+    def settle_near(i):
+        arrived(big.at[pl.ds(0, 3), rows_of(i)], sr.at[2 * i])
+
+    def settle_far(i):
+        arrived(chunk(i, diag), sr.at[2 * i + 1])
 
     def turn(w, wt):
         @pl.loop(0, tp)
@@ -160,20 +172,29 @@
 
     lane = lax.broadcasted_iota(jnp.int32, (cap, 128), 1)
 
-    def product(i, h, wt):
+    chips = (diag, nbr[0], nbr[1], me_t)
+
+    def product(i, h, wt, some):
+        total = None
+        for t in some:
+            for k in range(2):
+                j = lax.div(t, 2) * 2 + k
+                term = dot_nn(big[j, rows_of(i), halves[h]], wt[pl.ds(pl.multiple_of(j * dw, dw), dw), :])
+                total = term if total is None else total + term
+        return total
+
+    def near_x(i):
+        pg[...] = product(i, 0, wgt, chips[1:])
+        pu[...] = product(i, 0, wut, chips[1:])
+
+    def near_c(i):
+        ph[...] = product(i, 1, wdt, chips[1:])
+
+    def forward(i):
         at = rows_of(i)
-        total = dot_nn(big[0, at, halves[h]], wt[0:dw, :])
-        for j in range(1, tp):
-            total = total + dot_nn(big[j, at, halves[h]], wt[j * dw : (j + 1) * dw, :])
-        return total
-
-    def forward_x(i):
-        pg[...] = product(i, 0, wgt)
-        pu[...] = product(i, 0, wut)
-
-    def forward_c(i):
-        at = rows_of(i)
-        g, u, h = pg[...], pu[...], product(i, 1, wdt)
+        g = pg[...] + product(i, 0, wgt, chips[:1])
+        u = pu[...] + product(i, 0, wut, chips[:1])
+        h = ph[...] + product(i, 1, wdt, chips[:1])
         sig = jax.nn.sigmoid(g)
         act = g * sig
         hidden = (act * u).astype(BF16)
@@ -183,23 +204,23 @@
         dots = jnp.sum(hidden.astype(F32) * h, axis=1, keepdims=True)
         dcol[0:cap, :] = jnp.where(lane == i, dots, dcol[0:cap, :])
 
-    chips = (diag, nbr[0], nbr[1], me_t)
-
-    def pieces(i):
+    def pieces(i, lo=0, hi=4):
         at = rows_of(i)
-        for q in range(4):
+        for q in range(lo, hi):
             wide = pl.ds(pl.multiple_of(lax.div(chips[q], 2) * (2 * dw), 2 * dw), 2 * dw)
             both = dot_nn(gp[at, :], wg[:, wide]) + dot_nn(up[at, :], wu[:, wide])
             low, high = both[:, 0:dw], both[:, dw : 2 * dw]
             psib[i, q] = jnp.where(core == 0, high, low).astype(BF16)
             own_sum[i, q] = jnp.where(core == 0, low, high)
-        send(psib.at[i], rsib.at[i], br.at[i], me_e, sib)
-
-    def spread(i):
-        arrived(rsib.at[i], br.at[i])
-        for q in range(3):
+        part = pl.ds(lo, hi - lo)
+        send(psib.at[i, part], rsib.at[i, part], br.at[2 * i + (lo > 0)], me_e, sib)
+
+    def spread(i, lo=0, hi=4):
+        arrived(rsib.at[i, pl.ds(lo, hi - lo)], br.at[2 * i + (lo > 0)])
+        top = min(hi, 3)
+        for q in range(lo, top):
             pown[i, q] = (own_sum[i, q] + rsib[i, q].astype(F32)).astype(BF16)
-        for q in range(3):
+        for q in range(lo, top):
             send(pown.at[i, q], rown.at[i, q], rr.at[i], me_e, chips[q])
 
     def collect(i):
@@ -209,7 +230,7 @@
             total = total + rown[i, q].astype(F32)
         if i:
             tsum[rows_of(i), :] = total.astype(BF16)
-            send(tsum.at[rows_of(i)], back.at[rows_of(i)], zbr.at[0], partner(me_e, i), me_t)
+            send(tsum.at[rows_of(i)], back.at[rows_of(i)], zbr.at[i], partner(me_e, i), me_t)
         else:
             back[rows_of(i), :] = total.astype(BF16)
 
@@ -244,60 +265,77 @@
         copy.start()
     stage_a(0)
     dcol[...] = jnp.zeros_like(dcol)
-    comb_ref[...] = both.T.astype(BF16)
+    flat = both.T.astype(BF16)
+    for i in range(ep):
+        comb_ref[i] = flat[:, i * cap : (i + 1) * cap]
     for k, (w, wt) in enumerate(((wg, wgt), (wu, wut), (wd, wdt))):
         loads[k].wait()
         turn(w, wt)
     stage_b(0)
     stage_a(1)
+    settle_near(0)
+    near_x(0)
+    near_c(0)
     stage_c(0)
-    settle(0)
-    forward_x(0)
-    stage_b(1)
     if ep == 4:
-        forward_c(0)
         stage_a(3)
+        stage_b(1)
+        stage_a(2)
+        settle_far(0)
+        forward(0)
+        settle_near(1)
+        near_x(1)
+        stage_c(1)
+        near_c(1)
+        settle_far(1)
+        forward(1)
+        stage_b(3)
+        pieces(1)
+        stage_b(2)
+        settle_near(3)
+        near_x(3)
+        near_c(3)
+        stage_c(3)
+        spread(1)
         pieces(0)
-        stage_a(2)
-        stage_c(1)
-        settle(1)
-        forward_x(1)
-        stage_b(3)
-        forward_c(1)
-        stage_b(2)
-        pieces(1)
-        stage_c(3)
-        settle(3)
-        forward_x(3)
-        spread(1)
+        settle_far(3)
+        forward(3)
         stage_c(2)
-        forward_c(3)
         pieces(3)
-        settle(2)
-        forward_x(2)
+        spread(0)
+        settle_near(2)
+        near_x(2)
+        settle_far(2)
         spread(3)
-        forward_c(2)
+        near_c(2)
+        forward(2)
+        send_dots()
+        pieces(2, 0, 2)
+        pieces(2, 2, 4)
         collect(1)
-        send_dots()
-        pieces(2)
         flats()
-        weight_grad(gp_t, 0, ggo, 0, 4)
-        spread(2)
+        spread(2, 0, 2)
+        weight_grad(gp_t, 0, ggo, 0, 2)
+        spread(2, 2, 4)
+        weight_grad(gp_t, 0, ggo, 2, 8)
         collect(3)
         return_dots()
-        spread(0)
-        weight_grad(gp_t, 0, ggo, 4, 8)
+        collect(0)
         weight_grad(up_t, 0, ugo, 0, 8)
+        weight_grad(hid_t, 1, dgo, 0, 2)
         collect(2)
-        weight_grad(hid_t, 1, dgo, 0, 4)
-        collect(0)
-        weight_grad(hid_t, 1, dgo, 4, 8)
+        weight_grad(hid_t, 1, dgo, 2, 8)
+        last = 2
     else:
-        forward_c(0)
+        stage_b(1)
+        settle_far(0)
+        forward(0)
         stage_c(1)
-        settle(1)
-        forward_x(1)
-        forward_c(1)
+        settle_near(1)
+        near_x(1)
+        near_c(1)
+        settle_far(1)
+        forward(1)
         send_dots()
         pieces(1)
         pieces(0)
@@ -310,6 +348,12 @@
         collect(1)
         collect(0)
         weight_grad(hid_t, 1, dgo, 0, 8)
+        last = 1
+
+    def token_part(i):
+        if i:
+            arrived(back.at[rows_of(i)], zbr.at[i])
+        return dot_nn(comb_ref[i], back[rows_of(i), :])
 
     arrived(dback.at[pl.ds(1, ep - 1)], dzr.at[0])
     share = tok_dev // tp
@@ -331,8 +375,11 @@
     shares = jnp.concatenate([*grads, jnp.zeros((6, tok_dev), F32)], axis=0)
     gg_ref[...] = jnp.dot(shares, own_pick, precision=lax.Precision.HIGHEST, preferred_element_type=F32)[0:2, :]
 
-    arrived(back.at[pl.ds(cap, slots - cap)], zbr.at[0])
-    tg_ref[...] = dot_nn(comb_ref[...], back[...]).astype(BF16)
+    total = token_part(0)
+    for i in range(1, ep):
+        if i != last:
+            total = total + token_part(i)
+    tg_ref[...] = (total + token_part(last)).astype(BF16)
     for copy in sends:
         copy.wait_send()
 
@@ -369,9 +416,13 @@
     results = pl.pallas_call(
         functools.partial(exchange_kernel, ep, tp, cap),
         out_shape=tuple(pltpu.VMEM(*leaf) for leaf in small + grads),
-        in_specs=[vmem] * 4 + [any_] * 3,
+        in_specs=[any_] * 7,
         out_specs=[vmem] * 5,
         scratch_shapes=[
+            pltpu.VMEM((tok_dev, dw), BF16),
+            pltpu.VMEM((tok_dev, dw), BF16),
+            pltpu.VMEM((top_k, tok_dev), jnp.int32),
+            pltpu.VMEM((top_k, tok_dev), F32),
             pltpu.VMEM((fw, model), BF16),
             pltpu.VMEM((fw, model), BF16),
             pltpu.VMEM((fw, model), BF16),
@@ -380,8 +431,9 @@
             pltpu.VMEM((model, fw), BF16),
             pltpu.VMEM((slots, 2 * dw), BF16),
             pltpu.VMEM((tp, slots, 2 * dw), BF16),
-            pltpu.VMEM((tok_dev, slots), BF16),
+            pltpu.VMEM((ep, tok_dev, cap), BF16),
             pltpu.VMEM((2, slots, tok_dev), F32),
+            pltpu.VMEM((cap, fw), F32),
             pltpu.VMEM((cap, fw), F32),
             pltpu.VMEM((cap, fw), F32),
             pltpu.VMEM((slots, fw), BF16),
@@ -402,7 +454,8 @@
             pltpu.VMEM((tp - 1, 8, 128), F32),
             pltpu.VMEM((8, 128), F32),
             pltpu.VMEM((ep, 8, 128), F32),
-            dma(3), dma(1), dma(ep), dma(2 * ep), dma(ep), dma(ep), dma(ep), dma(ep), dma(1), dma(1), dma(1),
+            dma(4), dma(3), dma(1), dma(ep), dma(2 * ep), dma(ep), dma(2 * ep), dma(2 * ep), dma(ep), dma(ep),
+            dma(1), dma(1),
         ],
         compiler_params=pltpu.CompilerParams(
             collective_id=0, has_side_effects=True, vmem_limit_bytes=46 * MIB),

time: 47.7 us -> 45 us (0.943)
  Pallas kernels: 46.7 us -> 44.1 us
    pallas_call x1, Pallas kernels: 43.2 us -> 40.5 us  [fused(): pl.pallas_call(functools.partial(exchange_kernel, ep, tp, cap), out_shape...]
where the time goes in v3:
time: 45 us; the launch traced here: 44.9 us
  Pallas kernels  44.1 us (98%)
  between operations  0.8 us (2%)
    pallas_call x1, Pallas kernels, fused(): pl.pallas_call(functools.partial(exchange_kernel, ep, tp, cap), out_shape...  40.5 us
    pallas_call x1, Pallas kernels, fused(): pl.pallas_call(store_kernel, out_shape=tuple((jax.ShapeDtypeStruct(*leaf)...  3.53 us

profile of v3, /device:TPU:0, one launch (start us, length us, event | category | flops | bytes accessed | tf_op | source)
XLA Modules:
  0.0 44.9 jit_solution(15513107022211602808)
XLA Ops:
  0.6 40.5 %shard_map.110 = (bf16[128,256]{1,0:T(8,128)(2,1)S(1)}, f32[2,16]{1,0:T(2,128)S(1)}, bf16[704,2048]{1,0:T(8,128)(2,1)S(1)}, bf16[704,2048]{1,0:T(8,128)(2,1)S(1)}, bf16[704,2048]{1,0:T(8,128)(2,1)S(1)}) custom-call(bf16[128,256]{1,0:T(8,128)(2,1)} %tok_hbm.1, bf16[128,256]{1,0:T(8,128)(2,1)} %og_hbm.1, s32[2,128]{1,0:T(2,128)} %bitcast.11, ...), custom_call_target="tpu_custom_call" | custom-call | flops 8858370048 | bytes 8650752 | tf_op jit(solution)/shard_map/pallas_call | solution.py:416
  41.2 3.5 %shard_map.111 = (bf16[128,256]{1,0:T(8,128)(2,1)}, f32[2,16]{1,0:T(2,128)}, bf16[1,704,2048]{2,1,0:T(8,128)(2,1)}, bf16[1,704,2048]{2,1,0:T(8,128)(2,1)}, bf16[1,704,2048]{2,1,0:T(8,128)(2,1)}) custom-call(bf16[128,256]{1,0:T(8,128)(2,1)S(1)} %get-tuple-element.15.tg_ref, f32[2,16]{1,0:T(2,128)S(1)} %get-tuple-element.16.gg_ref, ...), custom_call_target="tpu_custom_call" | custom-call | flops 270336 | bytes 8650752 | tf_op jit(solution)/shard_map/pallas_call | solution.py:466

commit v4 on v3

--- a/solution.py
+++ b/solution.py
@@ -261,8 +261,7 @@
     z_order = (1, 3, 2) if ep == 4 else (1,)
     z_sends = [send_z(i) for i in z_order]
     sends.extend(z_sends)
-    for copy in z_sends:
-        copy.start()
+    z_sends[0].start()
     stage_a(0)
     dcol[...] = jnp.zeros_like(dcol)
     flat = both.T.astype(BF16)
@@ -271,6 +270,9 @@
     for k, (w, wt) in enumerate(((wg, wgt), (wu, wut), (wd, wdt))):
         loads[k].wait()
         turn(w, wt)
+        if k == 0:
+            for copy in z_sends[1:]:
+                copy.start()
     stage_b(0)
     stage_a(1)
     settle_near(0)
@@ -288,10 +290,10 @@
         stage_c(1)
         near_c(1)
         settle_far(1)
+        stage_b(3)
         forward(1)
-        stage_b(3)
+        stage_b(2)
         pieces(1)
-        stage_b(2)
         settle_near(3)
         near_x(3)
         near_c(3)
@@ -322,9 +324,8 @@
         return_dots()
         collect(0)
         weight_grad(up_t, 0, ugo, 0, 8)
-        weight_grad(hid_t, 1, dgo, 0, 2)
         collect(2)
-        weight_grad(hid_t, 1, dgo, 2, 8)
+        weight_grad(hid_t, 1, dgo, 0, 8)
         last = 2
     else:
         stage_b(1)

time: 45 us -> 43.9 us (0.976)
  Pallas kernels: 44.1 us -> 42.9 us
    pallas_call x1, Pallas kernels: 40.5 us -> 39.4 us  [fused(): pl.pallas_call(functools.partial(exchange_kernel, ep, tp, cap), out_shape...]
where the time goes in v4:
time: 43.9 us; the launch traced here: 43.7 us
  Pallas kernels  42.9 us (98%)
  between operations  0.8 us (2%)
    pallas_call x1, Pallas kernels, fused(): pl.pallas_call(functools.partial(exchange_kernel, ep, tp, cap), out_shape...  39.4 us
    pallas_call x1, Pallas kernels, fused(): pl.pallas_call(store_kernel, out_shape=tuple((jax.ShapeDtypeStruct(*leaf)...  3.53 us

profile of v4, /device:TPU:0, one launch (start us, length us, event | category | flops | bytes accessed | tf_op | source)
XLA Modules:
  0.0 43.7 jit_solution(2111132122252555256)
XLA Ops:
  0.6 39.4 %shard_map.110 = (bf16[128,256]{1,0:T(8,128)(2,1)S(1)}, f32[2,16]{1,0:T(2,128)S(1)}, bf16[704,2048]{1,0:T(8,128)(2,1)S(1)}, bf16[704,2048]{1,0:T(8,128)(2,1)S(1)}, bf16[704,2048]{1,0:T(8,128)(2,1)S(1)}) custom-call(bf16[128,256]{1,0:T(8,128)(2,1)} %tok_hbm.1, bf16[128,256]{1,0:T(8,128)(2,1)} %og_hbm.1, s32[2,128]{1,0:T(2,128)} %bitcast.11, ...), custom_call_target="tpu_custom_call" | custom-call | flops 8858370048 | bytes 8650752 | tf_op jit(solution)/shard_map/pallas_call | solution.py:417
  40.0 3.5 %shard_map.111 = (bf16[128,256]{1,0:T(8,128)(2,1)}, f32[2,16]{1,0:T(2,128)}, bf16[1,704,2048]{2,1,0:T(8,128)(2,1)}, bf16[1,704,2048]{2,1,0:T(8,128)(2,1)}, bf16[1,704,2048]{2,1,0:T(8,128)(2,1)}) custom-call(bf16[128,256]{1,0:T(8,128)(2,1)S(1)} %get-tuple-element.15.tg_ref, f32[2,16]{1,0:T(2,128)S(1)} %get-tuple-element.16.gg_ref, ...), custom_call_target="tpu_custom_call" | custom-call | flops 270336 | bytes 8650752 | tf_op jit(solution)/shard_map/pallas_call | solution.py:467
